TPU v7x, 128 devices: a whole 4x4x4 slice. The times are simulated.
128 devices in a mesh: sp: 32 (over z, y, core), tp: 4 (over x).
Axes of the slice: x: 4, y: 4, z: 4, core: 2. Of those that a mesh axis runs over, the one named last changes fastest.
Arguments:
- tokens: bfloat16 [6, 8192, 2048], P(None, 'sp', 'tp'), may hold values from -6 to 6
- norm_gains: float32 [3, 2048], replicated, may hold values from 0.5 to 1.5
- weight_outer: bfloat16 [3, 2048, 1024], P(None, 'sp', 'tp'), may hold values from -0.125 to 0.125
- weight_inner: bfloat16 [3, 2048, 1024], P(None, 'sp', 'tp'), may hold values from -0.125 to 0.125
- weight_value: bfloat16 [3, 2048, 1024], P(None, 'sp', 'tp'), may hold values from -0.125 to 0.125
- conv_taps: bfloat16 [3, 3, 1024], P(None, None, 'tp'), may hold values from -3.5 to 3.5
- weight_output: bfloat16 [3, 1024, 2048], P(None, 'sp', 'tp'), may hold values from -0.1875 to 0.1875
Outputs:
- mixed_out: float32 [6, 8192, 2048], P(None, 'sp', 'tp')
All inputs are finite; a program needn't handle non-finite values.
Results may differ from a plain program's by a relative error of at most 0.03.
Values may be sent and summed in bfloat16 or wider, within the bound.
No kernel may reach another device: no remote copies, remote signals or barrier semaphores. Data moves between devices by JAX's collectives and lax.ppermute only.
A program may use at most 128 MiB of HBM per device.

v0:
```python
import jax
import jax.numpy as jnp
from jax import lax
from jax.sharding import PartitionSpec as P

epsilon = 1e-06


def laid_out(parts, dim):
    dims = list(parts.shape[1:])
    dims[dim] *= parts.shape[0]
    return jnp.moveaxis(parts, 0, dim).reshape(dims)


def gather_packed(arrays, axis, dims):
    ravelled = jnp.concatenate([a.reshape(-1) for a in arrays])
    lines, at, finished = lax.all_gather(ravelled, axis), 0, []
    for a, dim in zip(arrays, dims):
        parts = lines[:, at : at + a.size].reshape(-1, *a.shape)
        finished.append(laid_out(parts, dim))
        at += a.size
    return tuple(finished)


def shifted(block, axis, distance):
    devices = range(lax.axis_size(axis))
    route = [(i - distance, i) for i in devices if i - distance in devices]
    return lax.ppermute(block, axis, route)


def normalize(values_in, gain_row):
    values = values_in.astype(jnp.float32)
    scale = lax.rsqrt(jnp.mean(values * values, axis=-1, keepdims=True) + epsilon)
    return (values * scale * gain_row.astype(jnp.float32)).astype(jnp.bfloat16)


def convolve(extended, taps):
    width = taps.shape[0]
    out_rows = extended.shape[1] - (width - 1)
    total = jnp.zeros((extended.shape[0], out_rows, extended.shape[2]), jnp.float32)
    for offset in range(width):
        total = total + taps[offset].astype(jnp.float32) * extended[:, offset : offset + out_rows]
    return total


def fetch_layer(weight_outer, weight_inner, weight_value, weight_output, layer):
    pieces = (weight_outer[layer], weight_inner[layer], weight_value[layer], weight_output[layer])
    return gather_packed((pieces[0], pieces[1], pieces[2], pieces[3]), "sp", (0, 0, 0, 0))


def body(tokens, norm_gains, weight_outer, weight_inner, weight_value, conv_taps, weight_output):
    layers = conv_taps.shape[0]
    history = conv_taps.shape[1] - 1
    sequences = tokens.shape[0]
    current = tokens
    upcoming = fetch_layer(weight_outer, weight_inner, weight_value, weight_output, 0)
    result = None
    for layer in range(layers):
        rows = current.shape[1]
        whole = lax.all_gather(current, "tp", axis=2, tiled=True)
        normed = normalize(whole, norm_gains[layer]).reshape(sequences * rows, whole.shape[2])
        gathered = upcoming
        if layer + 1 < layers:
            upcoming = fetch_layer(
                weight_outer, weight_inner, weight_value, weight_output, layer + 1
            )
        outer = jnp.dot(normed, gathered[0], preferred_element_type=jnp.float32)
        inner = jnp.dot(normed, gathered[1], preferred_element_type=jnp.float32)
        value = jnp.dot(normed, gathered[2], preferred_element_type=jnp.float32)
        outer = outer.astype(jnp.bfloat16)
        inner = inner.astype(jnp.bfloat16)
        value = value.astype(jnp.bfloat16)
        outer, inner, value = lax.optimization_barrier((outer, inner, value))
        channels = outer.shape[1]
        outer = outer.reshape(sequences, rows, channels)
        gated = (inner.astype(jnp.float32) * value.astype(jnp.float32)).reshape(
            sequences, rows, channels
        )
        earlier = shifted(gated[:, rows - history :], "sp", 1)
        extended = jnp.concatenate([earlier, gated], axis=1)
        kept = outer
        conved = convolve(extended, conv_taps[layer])
        mixer = (kept.astype(jnp.float32) * conved).astype(jnp.bfloat16)
        out_rows = mixer.shape[1]
        full_mix = lax.all_gather(mixer, "tp", axis=2, tiled=True)
        flat_mix = full_mix.reshape(sequences * out_rows, full_mix.shape[2])
        projected = jnp.dot(flat_mix, gathered[3], preferred_element_type=jnp.float32)
        result = projected.reshape(sequences, out_rows, projected.shape[1])
        current = result.astype(jnp.bfloat16)
    return result


def solution(mesh):
    in_specs = (
        P(None, "sp", "tp"),
        P(),
        P(None, "sp", "tp"),
        P(None, "sp", "tp"),
        P(None, "sp", "tp"),
        P(None, None, "tp"),
        P(None, "sp", "tp"),
    )
    out_specs = P(None, "sp", "tp")
    return jax.shard_map(body, mesh=mesh, in_specs=in_specs, out_specs=out_specs, check_vma=False)
```

profile of v0, /device:TPU:0, one launch (start us, length us, event | category | flops | bytes accessed | tf_op | source)
XLA Modules:
  0.0 554.1 jit_solution(3194071484672523936)
XLA Ops:
  6.5 0.8 slice_bitcast_fusion
  7.4 0.8 slice_bitcast_fusion.1
  8.2 0.8 slice_bitcast_fusion.2
  9.0 0.8 slice_bitcast_fusion.3
  9.8 0.7 pad_maximum_fusion.3
  10.6 0.7 all-gather.13.cloned.1.call-update
  11.3 0.9 fusion.33
  12.2 47.3 %all-gather.25.cloned.1.call-done = bf16[2097152]{0:T(1024)(128)(2,1)} async-done(((bf16[65536]{0:T(1024)(128)(2,1)}), bf16[2097152]{0:T(1024)(128)(2,1)}) %all-gather.25.cloned.1.call-update) | async-done | bytes 4194320 | tf_op jit(solution)/shard_map/all_gather | solution.py:17
  59.5 5.6 %reshape.102 = bf16[32,65536]{1,0:T(8,128)(2,1)} reshape(bf16[2097152]{0:T(1024)(128)(2,1)} %all-gather.25.cloned.1.call-done) | data formatting | bytes 8388608 | tf_op jit(solution)/shard_map/all_gather | solution.py:17
  65.0 3.4 fusion.32
  68.5 2.3 reshape_reshape.36
  70.8 1.3 reshape_reshape.37
  72.1 0.5 reshape_reshape.38
  72.6 53.4 %all-gather.13.cloned.1.call-done = bf16[6,256,2048]{2,1,0:T(8,128)(2,1)} async-done(((bf16[6,256,512]{2,1,0:T(8,128)(2,1)}), bf16[6,256,2048]{2,1,0:T(8,128)(2,1)}) %all-gather.13.cloned.1.call-update) | async-done | bytes 6291472 | tf_op jit(solution)/shard_map/all_gather | solution.py:60
  125.9 4.2 fusion
  130.2 0.4 copy-done
  130.5 1.5 fusion.2
  132.1 1.9 convolution_convert_fusion.8
  133.9 1.9 convolution_convert_fusion.7
  135.8 1.9 convolution_convert_fusion.6
  137.9 1.5 collective-permute-start
  139.4 0.8 collective-permute-done
  140.2 1.5 fusion.26
  141.9 0.7 pad_maximum_fusion.4
  142.8 0.5 reshape.105
  143.3 44.0 %all-gather.15.cloned.1.call-done = bf16[6,256,1024]{2,1,0:T(8,128)(2,1)} async-done(((bf16[6,256,256]{2,1,0:T(8,128)(2,1)}), bf16[6,256,1024]{2,1,0:T(8,128)(2,1)}) %all-gather.15.cloned.1.call-update) | async-done | bytes 3145744 | tf_op jit(solution)/shard_map/all_gather | solution.py:85
  187.3 4.8 convolution_convert_fusion.10
  192.2 44.5 %all-gather.27.cloned.1.call-done = bf16[2097152]{0:T(1024)(128)(2,1)} async-done(((bf16[65536]{0:T(1024)(128)(2,1)}), bf16[2097152]{0:T(1024)(128)(2,1)}) %all-gather.27.cloned.1.call-update) | async-done | bytes 4194320 | tf_op jit(solution)/shard_map/all_gather | solution.py:17
  236.7 5.6 %reshape.103 = bf16[32,65536]{1,0:T(8,128)(2,1)} reshape(bf16[2097152]{0:T(1024)(128)(2,1)} %all-gather.27.cloned.1.call-done) | data formatting | bytes 8388608 | tf_op jit(solution)/shard_map/all_gather | solution.py:17
  242.3 3.5 fusion.31
  245.8 2.3 reshape_reshape.40
  248.1 1.3 reshape_reshape.41
  249.4 0.5 reshape_reshape.42
  250.0 53.1 %all-gather.17.cloned.1.call-done = bf16[6,256,2048]{2,1,0:T(8,128)(2,1)} async-done(((bf16[6,256,512]{2,1,0:T(8,128)(2,1)}), bf16[6,256,2048]{2,1,0:T(8,128)(2,1)}) %all-gather.17.cloned.1.call-update) | async-done | bytes 6291472 | tf_op jit(solution)/shard_map/all_gather | solution.py:60
  303.0 4.2 fusion.3
  307.6 1.5 fusion.5
  309.1 1.9 convolution_convert_fusion.5
  311.0 1.9 convolution_convert_fusion.4
  312.9 1.9 convolution_convert_fusion.3
  314.9 1.7 collective-permute-start.1
  316.6 0.6 collective-permute-done.1
  317.2 1.5 fusion.20
  318.9 0.7 pad_maximum_fusion.5
  319.7 0.5 reshape.106
  320.2 44.2 %all-gather.19.cloned.1.call-done = bf16[6,256,1024]{2,1,0:T(8,128)(2,1)} async-done(((bf16[6,256,256]{2,1,0:T(8,128)(2,1)}), bf16[6,256,1024]{2,1,0:T(8,128)(2,1)}) %all-gather.19.cloned.1.call-update) | async-done | bytes 3145744 | tf_op jit(solution)/shard_map/all_gather | solution.py:85
  364.4 4.8 convolution_convert_fusion.9
  369.3 44.6 %all-gather.29.cloned.1.call-done = bf16[2097152]{0:T(1024)(128)(2,1)} async-done(((bf16[65536]{0:T(1024)(128)(2,1)}), bf16[2097152]{0:T(1024)(128)(2,1)}) %all-gather.29.cloned.1.call-update) | async-done | bytes 4194320 | tf_op jit(solution)/shard_map/all_gather | solution.py:17
  413.9 5.6 %reshape.104 = bf16[32,65536]{1,0:T(8,128)(2,1)} reshape(bf16[2097152]{0:T(1024)(128)(2,1)} %all-gather.29.cloned.1.call-done) | data formatting | bytes 8388608 | tf_op jit(solution)/shard_map/all_gather | solution.py:17
  419.5 3.5 fusion.30
  423.0 2.3 reshape_reshape.44
  425.3 1.3 reshape_reshape.45
  426.7 0.5 reshape_reshape.46
  427.2 53.2 %all-gather.21.cloned.1.call-done = bf16[6,256,2048]{2,1,0:T(8,128)(2,1)} async-done(((bf16[6,256,512]{2,1,0:T(8,128)(2,1)}), bf16[6,256,2048]{2,1,0:T(8,128)(2,1)}) %all-gather.21.cloned.1.call-update) | async-done | bytes 6291472 | tf_op jit(solution)/shard_map/all_gather | solution.py:60
  480.4 4.2 fusion.6
  485.0 1.5 fusion.8
  486.5 1.9 convolution_convert_fusion.2
  488.4 1.9 convolution_convert_fusion.1
  490.2 1.9 convolution_convert_fusion
  492.3 1.7 collective-permute-start.2
  494.1 0.6 collective-permute-done.2
  494.6 1.5 fusion.14
  496.1 0.5 reshape.107
  496.7 45.1 %all-gather.23.cloned.1.call-done = bf16[6,256,1024]{2,1,0:T(8,128)(2,1)} async-done(((bf16[6,256,256]{2,1,0:T(8,128)(2,1)}), bf16[6,256,1024]{2,1,0:T(8,128)(2,1)}) %all-gather.23.cloned.1.call-update) | async-done | bytes 3145744 | tf_op jit(solution)/shard_map/all_gather | solution.py:85
  541.8 5.4 fusion.34
  (58 shorter events, 2.2 us)
Async XLA Ops:
  6.5 53.0 %all-gather.25.cloned.1.call-start = ((), (), s32[]{:S(2)}) async-start(), calls=%async_computation.6 | async-start | bytes 4325376 | tf_op jit(solution)/shard_map/all_gather | solution.py:17
  10.5 115.4 %all-gather.13.cloned.1.call-start = ((), (), s32[]{:S(2)}) async-start(), calls=%async_computation | async-start | bytes 7864320 | tf_op jit(solution)/shard_map/all_gather | solution.py:60
  11.3 176.0 %all-gather.15.cloned.1.call-start = ((), (), s32[]{:S(2)}) async-start(), calls=%async_computation.1 | async-start | bytes 3932160 | tf_op jit(solution)/shard_map/all_gather | solution.py:85
  125.9 4.6 copy-start
  130.5 1.5 copy-start.7
  132.1 1.9 copy-start.8
  137.7 1.7 copy-start.9
  137.9 2.3 collective-permute-start
  141.7 95.0 %all-gather.27.cloned.1.call-start = ((), (), s32[]{:S(2)}) async-start(), calls=%async_computation.7 | async-start | bytes 4325376 | tf_op jit(solution)/shard_map/all_gather | solution.py:17
  142.6 160.5 %all-gather.17.cloned.1.call-start = ((), (), s32[]{:S(2)}) async-start(), calls=%async_computation.2 | async-start | bytes 7864320 | tf_op jit(solution)/shard_map/all_gather | solution.py:60
  192.2 172.2 %all-gather.19.cloned.1.call-start = ((), (), s32[]{:S(2)}) async-start(), calls=%async_computation.3 | async-start | bytes 3932160 | tf_op jit(solution)/shard_map/all_gather | solution.py:85
  303.0 4.6 copy-start.2
  307.6 1.5 copy-start.5
  309.1 1.9 copy-start.6
  314.9 2.3 collective-permute-start.1
  318.8 95.2 %all-gather.29.cloned.1.call-start = ((), (), s32[]{:S(2)}) async-start(), calls=%async_computation.8 | async-start | bytes 4325376 | tf_op jit(solution)/shard_map/all_gather | solution.py:17
  319.6 160.8 %all-gather.21.cloned.1.call-start = ((), (), s32[]{:S(2)}) async-start(), calls=%async_computation.4 | async-start | bytes 7864320 | tf_op jit(solution)/shard_map/all_gather | solution.py:60
  369.3 172.5 %all-gather.23.cloned.1.call-start = ((), (), s32[]{:S(2)}) async-start(), calls=%async_computation.5 | async-start | bytes 3932160 | tf_op jit(solution)/shard_map/all_gather | solution.py:85
  480.4 4.6 copy-start.1
  485.0 1.5 copy-start.3
  486.5 1.9 copy-start.4
  492.3 2.3 collective-permute-start.2
Sparse Core Ops, SparseCore 0:
  10.7 48.7 all-gather.24
  61.2 64.7 all-gather.12
  141.8 45.4 all-gather.14
  189.5 47.2 all-gather.26
  238.2 64.7 all-gather.16
  318.9 45.4 all-gather.18
  366.7 47.2 all-gather.28
  415.6 64.7 all-gather.20
  496.2 45.4 all-gather.22
where the time goes:
time: 563 us; the launch traced here: 554 us
  waiting for transfers between devices  432 us (77%)
  local copies, waits for them, and re-layouts  46.6 us (8%)
  matrix products  31.7 us (6%)
  other arithmetic  24.2 us (4%)
  between operations  14.1 us (3%)
    all_gather x3, waiting for transfers between devices, body(): whole = lax.all_gather(current, 'tp', axis=2, tiled=True)  160 us
    all_gather x3, waiting for transfers between devices, gather_packed(): lines, at, finished = (lax.all_gather(ravelled, axis), 0, [])  136 us
    all_gather x3, waiting for transfers between devices, body(): full_mix = lax.all_gather(mixer, 'tp', axis=2, tiled=True)  133 us
    all_gather x3, local copies, waits for them, and re-layouts, gather_packed(): lines, at, finished = (lax.all_gather(ravelled, axis), 0, [])  16.7 us
    dot_general x3, matrix products, body(): jnp.dot(flat_mix, gathered[3], preferred_element_type=jnp.float32)  15 us
    another operation x12, local copies, waits for them, and re-layouts, laid_out(): return jnp.moveaxis(parts, 0, dim).reshape(dims)  14 us
    reduce_sum x3, other arithmetic, normalize(): jnp.mean(values * values, axis=-1, keepdims=True) + epsilon  12.7 us
  transfers between devices with their start and end apart: 12, of which 12 were waited for; matrix products, arithmetic and copies ran while one was open for 10% of the time, Pallas kernels for 0%

commit v1 on v0

v1 whole, which is shorter than its diff:
```python
import jax
import jax.numpy as jnp
from jax import lax
from jax.experimental import pallas as pl
from jax.experimental.pallas import tpu as pltpu
from jax.sharding import PartitionSpec as P

epsilon = 1e-06

SEQS, D, SC, LAYERS, KERNEL = 6, 2048, 1024, 3, 3
SP, TP = 32, 4
HALO = 8
OWN = 64
SPAN = OWN + HALO
ROWS = SEQS * SPAN
KIN, KOUT = D // SP, SC // SP
CB = SC // TP
FB = D // TP
PACK = LAYERS * 4 * KIN
TAPROWS = 16


def layers_kernel(x_ref, gains_ref, taps_ref, g_ref, out_ref, win, wout, cur, normed, mixer, sem_in, sem_out):
    def in_copies(layer, x):
        slot = layer % 2
        return [
            pltpu.make_async_copy(
                g_ref.at[:, x, pl.ds((layer * 4 + m) * KIN, KIN), :],
                win.at[slot, m, :, :, pl.ds(x * CB, CB)],
                sem_in.at[slot, x, m],
            )
            for m in range(3)
        ]

    def out_copies(layer, x):
        slot = layer % 2
        return [
            pltpu.make_async_copy(
                g_ref.at[:, x, pl.ds((layer * 4 + 3) * KIN + h * KOUT, KOUT), :],
                wout.at[slot, :, :, pl.ds(x * FB + h * CB, CB)],
                sem_out.at[slot, x, h],
            )
            for h in range(2)
        ]

    def start_in(layer):
        for x in range(TP):
            for c in in_copies(layer, x):
                c.start()

    def start_out(layer):
        for x in range(TP):
            for c in out_copies(layer, x):
                c.start()

    start_in(0)
    start_out(0)
    start_in(1)
    start_out(1)
    for x in range(TP):
        cur[:, x * FB : (x + 1) * FB] = x_ref[x]

    for layer in range(LAYERS):
        slot = layer % 2

        @pl.loop(0, ROWS // 16)
        def _(r):
            rows = pl.ds(pl.multiple_of(r * 16, 16), 16)
            v = cur[rows, :].astype(jnp.float32)
            scale = lax.rsqrt(jnp.sum(v * v, axis=-1, keepdims=True) * (1.0 / D) + epsilon)
            normed[rows, :] = (v * scale * gains_ref[layer : layer + 1, :]).astype(jnp.bfloat16)

        for x in range(TP):
            for c in in_copies(layer, x):
                c.wait()
            parts = []
            for m in range(3):
                w = win[slot, m, :, :, x * CB : (x + 1) * CB].reshape(D, CB)
                parts.append(
                    jnp.dot(normed[...], w, preferred_element_type=jnp.float32)
                    .astype(jnp.bfloat16)
                    .astype(jnp.float32)
                )
            outer, inner, value = parts
            gated = inner * value
            taps = taps_ref[x, layer * KERNEL : (layer + 1) * KERNEL, :].astype(jnp.float32)
            conved = taps[0:1] * pltpu.roll(gated, 2, 0)
            conved = conved + taps[1:2] * pltpu.roll(gated, 1, 0)
            conved = conved + taps[2:3] * gated
            mixer[:, x * CB : (x + 1) * CB] = (outer * conved).astype(jnp.bfloat16)
        if layer + 2 < LAYERS:
            start_in(layer + 2)

        for x in range(TP):
            for c in out_copies(layer, x):
                c.wait()
            w = wout[slot, :, :, x * FB : (x + 1) * FB].reshape(SC, FB)
            y = jnp.dot(mixer[...], w, preferred_element_type=jnp.float32)
            if layer + 1 < LAYERS:
                cur[:, x * FB : (x + 1) * FB] = y.astype(jnp.bfloat16)
            else:
                out_ref[x] = y.reshape(SEQS, SPAN, FB)[:, HALO:, :].astype(jnp.bfloat16)
        if layer + 2 < LAYERS:
            start_out(layer + 2)


def run_layers(x, gains, taps, g):
    flops = LAYERS * 2 * ROWS * SC * D * 4
    return pl.pallas_call(
        layers_kernel,
        out_shape=jax.ShapeDtypeStruct((TP, SEQS, OWN, FB), jnp.bfloat16),
        in_specs=[pl.BlockSpec(memory_space=pltpu.VMEM)] * 3 + [pl.BlockSpec(memory_space=pl.ANY)],
        out_specs=pl.BlockSpec(memory_space=pltpu.VMEM),
        scratch_shapes=[
            pltpu.VMEM((2, 3, SP, KIN, SC), jnp.bfloat16),
            pltpu.VMEM((2, SP, KOUT, D), jnp.bfloat16),
            pltpu.VMEM((ROWS, D), jnp.bfloat16),
            pltpu.VMEM((ROWS, D), jnp.bfloat16),
            pltpu.VMEM((ROWS, SC), jnp.bfloat16),
            pltpu.SemaphoreType.DMA((2, TP, 3)),
            pltpu.SemaphoreType.DMA((2, TP, 2)),
        ],
        compiler_params=pltpu.CompilerParams(vmem_limit_bytes=60 * 1024 * 1024),
        cost_estimate=pl.CostEstimate(flops=flops, bytes_accessed=48 * 1024 * 1024, transcendentals=0),
        name="mixer_layers",
    )(x, gains, taps, g)


def body(tokens, norm_gains, weight_outer, weight_inner, weight_value, conv_taps, weight_output):
    halves = jnp.stack([weight_output[:, :, :CB], weight_output[:, :, CB:]], axis=1).reshape(LAYERS, 1, KIN, CB)
    packed = jnp.concatenate(
        [jnp.stack([weight_outer, weight_inner, weight_value], axis=1), halves], axis=1
    ).reshape(PACK, CB)
    taps = jnp.pad(conv_taps.reshape(LAYERS * KERNEL, CB), ((0, TAPROWS - LAYERS * KERNEL), (0, 0)))
    packed = jnp.concatenate([packed, taps], axis=0)
    g = lax.all_gather(packed, ("sp", "tp")).reshape(SP, TP, PACK + TAPROWS, CB)

    before = lax.ppermute(tokens[:, -HALO:], "sp", [(i, i + 1) for i in range(SP - 1)])
    extended = jnp.concatenate([before, tokens], axis=1)
    send = jnp.stack([extended[:, i * OWN : i * OWN + SPAN] for i in range(TP)])
    x = lax.all_to_all(send, "tp", split_axis=0, concat_axis=0).reshape(TP, ROWS, FB)

    out = run_layers(x, norm_gains, g[0, :, PACK:, :], g)
    back = lax.all_to_all(out, "tp", split_axis=0, concat_axis=0)
    return jnp.moveaxis(back, 0, 1).reshape(SEQS, TP * OWN, FB).astype(jnp.float32)


def solution(mesh):
    in_specs = (
        P(None, "sp", "tp"),
        P(),
        P(None, "sp", "tp"),
        P(None, "sp", "tp"),
        P(None, "sp", "tp"),
        P(None, None, "tp"),
        P(None, "sp", "tp"),
    )
    return jax.shard_map(body, mesh=mesh, in_specs=in_specs, out_specs=P(None, "sp", "tp"), check_vma=False)
```

time: 563 us -> 237 us (0.42); the launches traced: 554 us -> 237 us
  waiting for transfers between devices: 432 us -> 137 us
  Pallas kernels: 0 us -> 45.6 us
  local copies, waits for them, and re-layouts: 46.6 us -> 5.56 us
  matrix products: 31.7 us -> 0 us
  blocking collectives: 0 us -> 25.4 us
  other arithmetic: 24.2 us -> 3.87 us
    all_gather x9 -> x1, waiting for transfers between devices: 429 us -> 136 us  [body(): g = lax.all_gather(packed, ('sp', 'tp')).reshape(SP, TP, PACK + TAPROWS, CB)]
    pallas_call x0 -> x1, Pallas kernels: none -> 45.6 us  [run_layers(): pl.pallas_call(layers_kernel, out_shape=jax.ShapeDtypeStruct((TP, SEQS, O...]
    dot_general x12 -> x0, matrix products: 31.7 us -> none  [the longest x3 15 us: body(): jnp.dot(flat_mix, gathered[3], preferred_element_type=jnp.float32)]
    all_to_all x0 -> x1, blocking collectives: none -> 25.4 us  [body(): back = lax.all_to_all(out, 'tp', split_axis=0, concat_axis=0)]
    all_gather x3 -> x0, local copies, waits for them, and re-layouts: 16.7 us -> none  [gather_packed(): lines, at, finished = (lax.all_gather(ravelled, axis), 0, [])]
    another operation x12 -> x1, local copies, waits for them, and re-layouts: 14 us -> 0.95 us  [body(): jnp.stack([weight_output[:, :, :CB], weight_output[:, :, CB:]], axis=1)]
    reduce_sum x3 -> x0, other arithmetic: 12.7 us -> none  [normalize(): jnp.mean(values * values, axis=-1, keepdims=True) + epsilon]
    slice x7 -> x1, local copies, waits for them, and re-layouts: 11.4 us -> 0.01 us  [body(): tokens[:, -HALO:]]
  transfers between devices with their start and end apart: 12 -> 3, of which waited for: 12 -> 2; matrix products, arithmetic and copies ran while one was open for 10% -> 1% of each run, Pallas kernels for 0% -> 0%
where the time goes in v1:
time: 237 us
  waiting for transfers between devices  137 us (58%)
  Pallas kernels  45.6 us (19%)
  blocking collectives  25.4 us (11%)
  between operations  13.5 us (6%)
  starting transfers between devices  6.18 us (3%)
  local copies, waits for them, and re-layouts  5.56 us (2%)
  other arithmetic  3.87 us (2%)
    all_gather x1, waiting for transfers between devices, body(): g = lax.all_gather(packed, ('sp', 'tp')).reshape(SP, TP, PACK + TAPROWS, CB)  136 us
    pallas_call x1, Pallas kernels, run_layers(): pl.pallas_call(layers_kernel, out_shape=jax.ShapeDtypeStruct((TP, SEQS, O...  45.6 us
    all_to_all x1, blocking collectives, body(): back = lax.all_to_all(out, 'tp', split_axis=0, concat_axis=0)  25.4 us
    all_to_all x1, starting transfers between devices, body(): lax.all_to_all(send, 'tp', split_axis=0, concat_axis=0)  4.89 us
  transfers between devices with their start and end apart: 3, of which 2 were waited for; matrix products, arithmetic and copies ran while one was open for 1% of the time, Pallas kernels for 0%

profile of v1, /device:TPU:0, one launch (start us, length us, event | category | flops | bytes accessed | tf_op | source)
XLA Modules:
  0.0 236.9 jit_solution(14926012084089971643)
XLA Ops:
  6.5 0.0 copy-start.2
  6.5 0.0 copy-start
  6.5 0.0 all-gather.3.cloned.1.call-start
  6.5 0.9 slice_bitcast_fusion.4
  7.5 1.0 pad_maximum_fusion.2
  8.6 0.0 copy-done.2
  8.6 0.8 fusion.2
  9.4 0.0 all-gather.3.cloned.1.call-update
  9.4 0.0 copy-done
  9.4 1.3 collective-permute-start
  10.7 0.9 collective-permute-done
  11.6 0.2 fusion.1
  11.8 1.4 pad_maximum_fusion
  13.2 4.9 %all-to-all-start = ((bf16[4,6,72,512]{3,2,1,0:T(8,128)(2,1)}), bf16[4,6,72,512]{3,2,1,0:T(8,128)(2,1)S(1)}, u32[]{:S(2)}, u32[]{:S(2)}) async-start(bf16[4,6,72,512]{3,2,1,0:T(8,128)(2,1)} %pad_maximum_fusion), calls=%async_computation | async-start | bytes 3538944 | tf_op jit(solution)/shard_map/all_to_all | solution.py:141
  18.1 135.9 %all-gather.3.cloned.1.call-done = bf16[100352,256]{1,0:T(8,128)(2,1)} async-done(((bf16[784,256]{1,0:T(8,128)(2,1)}), bf16[100352,256]{1,0:T(8,128)(2,1)}) %all-gather.3.cloned.1.call-update) | async-done | bytes 51380240 | tf_op jit(solution)/shard_map/all_gather | solution.py:136
  154.0 1.4 slice_bitcast_fusion.5.taps_ref
  155.4 0.0 all-to-all-done
  155.4 0.0 copy-start.1
  155.4 1.2 copy-done.1
  156.6 45.6 %mixer_layers.1 = bf16[4,6,64,512]{3,2,1,0:T(8,128)(2,1)} custom-call(bf16[4,432,512]{2,1,0:T(8,128)(2,1)} %bitcast.24, f32[3,2048]{1,0:T(4,128)} %gains_ref.1, bf16[4,16,256]{2,1,0:T(8,128)(2,1)} %slice_bitcast_fusion.5.taps_ref, bf16[32,4,784,256]{3,2,1,0:T(8,128)(2,1)} %bitcast.31), custom_call_target="tpu_custom_call" | custom-call | flops 21743271936 | bytes 50331648 | tf_op jit(solution)/shard_map/mixer_layers/pallas_call | solution.py:109
  202.2 25.4 %all_to_all.10 = bf16[4,6,64,512]{3,2,1,0:T(8,128)(2,1)S(1)} all-to-all(bf16[4,6,64,512]{3,2,1,0:T(8,128)(2,1)} %mixer_layers.1), channel_id=1, replica_groups=mesh['sp'=32,'tp'=4] {'tp'}, dimensions={0} | all-to-all | bytes 3145728 | tf_op jit(solution)/shard_map/all_to_all | solution.py:144
  227.6 0.4 convert_bitcast_fusion
  228.1 2.0 copy.9
  (4 shorter events, 0.1 us)
Async XLA Ops:
  6.5 2.1 copy-start.2
  6.5 2.9 %copy-start = (bf16[6,256,512]{2,1,0:T(8,128)(2,1)S(1)}, bf16[6,256,512]{2,1,0:T(8,128)(2,1)}, u32[]{:S(2)}) copy-start(bf16[6,256,512]{2,1,0:T(8,128)(2,1)} %param.7) | copy-start | bytes 4718596
  6.5 147.5 %all-gather.3.cloned.1.call-start = ((), (), s32[]{:S(2)}) async-start(), calls=%async_computation.2 | async-start | bytes 51781632 | tf_op jit(solution)/shard_map/all_gather | solution.py:136
  9.4 2.2 collective-permute-start
  13.2 142.2 %all-to-all-start = ((bf16[4,6,72,512]{3,2,1,0:T(8,128)(2,1)}), bf16[4,6,72,512]{3,2,1,0:T(8,128)(2,1)S(1)}, u32[]{:S(2)}, u32[]{:S(2)}) async-start(bf16[4,6,72,512]{3,2,1,0:T(8,128)(2,1)} %pad_maximum_fusion), calls=%async_computation | async-start | bytes 3538944 | tf_op jit(solution)/shard_map/all_to_all | solution.py:141
  155.4 1.2 copy-start.1
Sparse Core Ops, SparseCore 0:
  10.3 143.6 all-gather.2

commit v2 on v1

--- a/solution.py
+++ b/solution.py
@@ -20,7 +20,7 @@
 TAPROWS = 16
 
 
-def layers_kernel(x_ref, gains_ref, taps_ref, g_ref, out_ref, win, wout, cur, normed, mixer, sem_in, sem_out):
+def layers_kernel(x_ref, gains_ref, taps_ref, g_ref, out_ref, win, wout, xg, mixer, sem_in, sem_out):
     def in_copies(layer, x):
         slot = layer % 2
         return [
@@ -57,18 +57,17 @@
     start_out(0)
     start_in(1)
     start_out(1)
+    sumsq = jnp.zeros((ROWS, 128), jnp.float32)
     for x in range(TP):
-        cur[:, x * FB : (x + 1) * FB] = x_ref[x]
+        v = x_ref[x].astype(jnp.float32)
+        xg[:, x * FB : (x + 1) * FB] = (v * gains_ref[0:1, x * FB : (x + 1) * FB]).astype(jnp.bfloat16)
+        for i in range(FB // 128):
+            part = v[:, i * 128 : (i + 1) * 128]
+            sumsq = sumsq + part * part
 
     for layer in range(LAYERS):
         slot = layer % 2
-
-        @pl.loop(0, ROWS // 16)
-        def _(r):
-            rows = pl.ds(pl.multiple_of(r * 16, 16), 16)
-            v = cur[rows, :].astype(jnp.float32)
-            scale = lax.rsqrt(jnp.sum(v * v, axis=-1, keepdims=True) * (1.0 / D) + epsilon)
-            normed[rows, :] = (v * scale * gains_ref[layer : layer + 1, :]).astype(jnp.bfloat16)
+        scale = lax.rsqrt(jnp.sum(sumsq, axis=-1, keepdims=True) * (1.0 / D) + epsilon)
 
         for x in range(TP):
             for c in in_copies(layer, x):
@@ -76,11 +75,7 @@
             parts = []
             for m in range(3):
                 w = win[slot, m, :, :, x * CB : (x + 1) * CB].reshape(D, CB)
-                parts.append(
-                    jnp.dot(normed[...], w, preferred_element_type=jnp.float32)
-                    .astype(jnp.bfloat16)
-                    .astype(jnp.float32)
-                )
+                parts.append(jnp.dot(xg[...], w, preferred_element_type=jnp.float32) * scale)
             outer, inner, value = parts
             gated = inner * value
             taps = taps_ref[x, layer * KERNEL : (layer + 1) * KERNEL, :].astype(jnp.float32)
@@ -91,13 +86,18 @@
         if layer + 2 < LAYERS:
             start_in(layer + 2)
 
+        sumsq = jnp.zeros((ROWS, 128), jnp.float32)
         for x in range(TP):
             for c in out_copies(layer, x):
                 c.wait()
             w = wout[slot, :, :, x * FB : (x + 1) * FB].reshape(SC, FB)
             y = jnp.dot(mixer[...], w, preferred_element_type=jnp.float32)
             if layer + 1 < LAYERS:
-                cur[:, x * FB : (x + 1) * FB] = y.astype(jnp.bfloat16)
+                gains = gains_ref[layer + 1 : layer + 2, x * FB : (x + 1) * FB]
+                xg[:, x * FB : (x + 1) * FB] = (y * gains).astype(jnp.bfloat16)
+                for i in range(FB // 128):
+                    part = y[:, i * 128 : (i + 1) * 128]
+                    sumsq = sumsq + part * part
             else:
                 out_ref[x] = y.reshape(SEQS, SPAN, FB)[:, HALO:, :].astype(jnp.bfloat16)
         if layer + 2 < LAYERS:
@@ -114,7 +114,6 @@
         scratch_shapes=[
             pltpu.VMEM((2, 3, SP, KIN, SC), jnp.bfloat16),
             pltpu.VMEM((2, SP, KOUT, D), jnp.bfloat16),
-            pltpu.VMEM((ROWS, D), jnp.bfloat16),
             pltpu.VMEM((ROWS, D), jnp.bfloat16),
             pltpu.VMEM((ROWS, SC), jnp.bfloat16),
             pltpu.SemaphoreType.DMA((2, TP, 3)),

time: 237 us -> 229 us (0.966)
  Pallas kernels: 45.6 us -> 37.7 us
    pallas_call x1, Pallas kernels: 45.6 us -> 37.7 us  [run_layers(): pl.pallas_call(layers_kernel, out_shape=jax.ShapeDtypeStruct((TP, SEQS, O...]
where the time goes in v2:
time: 229 us
  waiting for transfers between devices  137 us (60%)
  Pallas kernels  37.7 us (16%)
  blocking collectives  25.4 us (11%)
  between operations  13.5 us (6%)
  starting transfers between devices  6.18 us (3%)
  local copies, waits for them, and re-layouts  5.56 us (2%)
  other arithmetic  3.87 us (2%)
    all_gather x1, waiting for transfers between devices, body(): g = lax.all_gather(packed, ('sp', 'tp')).reshape(SP, TP, PACK + TAPROWS, CB)  136 us
    pallas_call x1, Pallas kernels, run_layers(): pl.pallas_call(layers_kernel, out_shape=jax.ShapeDtypeStruct((TP, SEQS, O...  37.7 us
    all_to_all x1, blocking collectives, body(): back = lax.all_to_all(out, 'tp', split_axis=0, concat_axis=0)  25.4 us
    all_to_all x1, starting transfers between devices, body(): lax.all_to_all(send, 'tp', split_axis=0, concat_axis=0)  4.89 us
  transfers between devices with their start and end apart: 3, of which 2 were waited for; matrix products, arithmetic and copies ran while one was open for 1% of the time, Pallas kernels for 0%

profile of v2, /device:TPU:0, one launch (start us, length us, event | category | flops | bytes accessed | tf_op | source)
XLA Modules:
  0.0 229.0 jit_solution(10866084624253587675)
XLA Ops:
  6.5 0.0 copy-start.2
  6.5 0.0 copy-start
  6.5 0.0 all-gather.3.cloned.1.call-start
  6.5 0.9 slice_bitcast_fusion.4
  7.5 1.0 pad_maximum_fusion.2
  8.6 0.0 copy-done.2
  8.6 0.8 fusion.2
  9.4 0.0 all-gather.3.cloned.1.call-update
  9.4 0.0 copy-done
  9.4 1.3 collective-permute-start
  10.7 0.9 collective-permute-done
  11.6 0.2 fusion.1
  11.8 1.4 pad_maximum_fusion
  13.2 4.9 %all-to-all-start = ((bf16[4,6,72,512]{3,2,1,0:T(8,128)(2,1)}), bf16[4,6,72,512]{3,2,1,0:T(8,128)(2,1)S(1)}, u32[]{:S(2)}, u32[]{:S(2)}) async-start(bf16[4,6,72,512]{3,2,1,0:T(8,128)(2,1)} %pad_maximum_fusion), calls=%async_computation | async-start | bytes 3538944 | tf_op jit(solution)/shard_map/all_to_all | solution.py:140
  18.1 135.9 %all-gather.3.cloned.1.call-done = bf16[100352,256]{1,0:T(8,128)(2,1)} async-done(((bf16[784,256]{1,0:T(8,128)(2,1)}), bf16[100352,256]{1,0:T(8,128)(2,1)}) %all-gather.3.cloned.1.call-update) | async-done | bytes 51380240 | tf_op jit(solution)/shard_map/all_gather | solution.py:135
  154.0 1.4 slice_bitcast_fusion.5.taps_ref
  155.4 0.0 all-to-all-done
  155.4 0.0 copy-start.1
  155.4 1.2 copy-done.1
  156.6 37.7 %mixer_layers.1 = bf16[4,6,64,512]{3,2,1,0:T(8,128)(2,1)} custom-call(bf16[4,432,512]{2,1,0:T(8,128)(2,1)} %bitcast.24, f32[3,2048]{1,0:T(4,128)} %gains_ref.1, bf16[4,16,256]{2,1,0:T(8,128)(2,1)} %slice_bitcast_fusion.5.taps_ref, bf16[32,4,784,256]{3,2,1,0:T(8,128)(2,1)} %bitcast.31), custom_call_target="tpu_custom_call" | custom-call | flops 21743271936 | bytes 50331648 | tf_op jit(solution)/shard_map/mixer_layers/pallas_call | solution.py:109
  194.3 25.4 %all_to_all.10 = bf16[4,6,64,512]{3,2,1,0:T(8,128)(2,1)S(1)} all-to-all(bf16[4,6,64,512]{3,2,1,0:T(8,128)(2,1)} %mixer_layers.1), channel_id=1, replica_groups=mesh['sp'=32,'tp'=4] {'tp'}, dimensions={0} | all-to-all | bytes 3145728 | tf_op jit(solution)/shard_map/all_to_all | solution.py:143
  219.7 0.4 convert_bitcast_fusion
  220.2 2.0 copy.9
  (4 shorter events, 0.1 us)
Async XLA Ops:
  6.5 2.1 copy-start.2
  6.5 2.9 %copy-start = (bf16[6,256,512]{2,1,0:T(8,128)(2,1)S(1)}, bf16[6,256,512]{2,1,0:T(8,128)(2,1)}, u32[]{:S(2)}) copy-start(bf16[6,256,512]{2,1,0:T(8,128)(2,1)} %param.7) | copy-start | bytes 4718596
  6.5 147.5 %all-gather.3.cloned.1.call-start = ((), (), s32[]{:S(2)}) async-start(), calls=%async_computation.2 | async-start | bytes 51781632 | tf_op jit(solution)/shard_map/all_gather | solution.py:135
  9.4 2.2 collective-permute-start
  13.2 142.2 %all-to-all-start = ((bf16[4,6,72,512]{3,2,1,0:T(8,128)(2,1)}), bf16[4,6,72,512]{3,2,1,0:T(8,128)(2,1)S(1)}, u32[]{:S(2)}, u32[]{:S(2)}) async-start(bf16[4,6,72,512]{3,2,1,0:T(8,128)(2,1)} %pad_maximum_fusion), calls=%async_computation | async-start | bytes 3538944 | tf_op jit(solution)/shard_map/all_to_all | solution.py:140
  155.4 1.2 copy-start.1
Sparse Core Ops, SparseCore 0:
  10.3 143.6 all-gather.2
